TPU v7x, 512 devices: a 4x2x32 block of a 4x8x32 slice. The times are simulated.
512 devices in a mesh: grp: 2 (over y), sp: 64 (over z, core), tp: 4 (over x).
Axes of the slice: x: 4, y: 2, z: 32, core: 2. Of those that a mesh axis runs over, the one named last changes fastest.
The devices are a block of a 4x8x32 slice.
Arguments:
- tokens: bfloat16 [32768, 2048], P(('grp', 'sp'), 'tp'), parts along dimension 0, may hold values from -6 to 6
- norm_gain: float32 [2048], replicated, may hold values from 0.1 to 1.9
- ret_query_weight: bfloat16 [2048, 256], P('sp', 'tp'), may hold values from -0.125 to 0.125
- ret_key_weight: bfloat16 [2048, 256], P('sp', 'tp'), may hold values from -0.125 to 0.125
- ret_value_weight: bfloat16 [2048, 512], P('sp', 'tp'), may hold values from -0.125 to 0.125
- fox_query_weight: bfloat16 [2048, 512], P('sp', 'tp'), may hold values from -8 to 8
- fox_key_weight: bfloat16 [2048, 512], P('sp', 'tp'), may hold values from -0.125 to 0.125
- fox_value_weight: bfloat16 [2048, 512], P('sp', 'tp'), may hold values from -0.125 to 0.125
- ret_decay: float32 [8], P('tp'), may hold values from -1 to 0, as said below
- ret_state: float32 [16, 32, 64], P(('grp', 'tp')), parts along dimension 0, may hold values from -256 to 256
- head_norm_gain: float32 [512], P('tp'), may hold values from 0.1 to 1.9
- fox_gates: float32 [32768, 8], P('grp', 'tp'), parts along dimension 0, may hold values from -49152 to 0, as said below
- ret_out_weight: bfloat16 [512, 2048], P('tp', 'sp'), may hold values from -0.1875 to 0.1875
- fox_out_weight: bfloat16 [512, 2048], P('tp', 'sp'), may hold values from -1 to 1
Outputs:
- mixed: bfloat16 [32768, 2048], P(('grp', 'sp', 'tp')), parts along dimension 0
There are 2 independent parts, one for each index of `grp`. A program takes and returns all parts, laid end to end along the dimension named above; an argument that names none is the same for every part. Nothing has to cross between parts.
Inputs may be any that keep to these rules, and one draw needn't show every extreme that they name: `ret_decay`: each head's log decay is negative. `fox_gates`: along the positions each head's column never rises.
All inputs are finite; a program needn't handle non-finite values.
Results may differ from a plain program's by a relative error of at most 0.015.
The roundings to bfloat16 on the way count: a program that leaves them out, or rounds other values in their place, can miss the bound.
Values may be sent and summed in bfloat16 or wider, within the bound.
No kernel may reach another device: no remote copies, remote signals or barrier semaphores. Data moves between devices by JAX's collectives and lax.ppermute only.
A program may use at most 64 MiB of HBM per device.

v0:
```python
import jax
import jax.numpy as jnp
from jax import lax
from jax.sharding import Mesh
from jax.sharding import PartitionSpec as P

SP = ("sp_0", "sp_1")
GRP_SP = ("grp", "sp_0", "sp_1")
GRP_SP_TP = ("grp", "sp_0", "sp_1", "tp")
epsilon = 1e-06


def in_order(blocks, dim):
    shape = list(blocks.shape[1:])
    shape[dim] *= blocks.shape[0]
    return jnp.moveaxis(blocks, 0, dim).reshape(shape)


def from_everyone(array, axis):
    count = lax.axis_size(axis)
    return lax.all_to_all(
        jnp.broadcast_to(array[None], (count, *array.shape)), axis, 0, 0, tiled=True
    )


def collect_2(array, axis, dim):
    return in_order(from_everyone(array, axis), dim)


def sent_together(arrays, axis, dim, along):
    widths = [a.shape[along] for a in arrays]
    both = jnp.concatenate(arrays, axis=along)
    result = lax.all_gather(both, axis, axis=dim, tiled=True)
    return tuple(jnp.split(result, [sum(widths[:k]) for k in range(1, len(widths))], axis=along))


def all_blocks(array, axes, order):
    blocks = array
    for k in order:
        blocks = lax.all_gather(blocks, axes[k])
    done = order[::-1]
    back = [done.index(k) for k in range(len(axes))]
    blocks = blocks.transpose(*back, *range(len(axes), blocks.ndim))
    return blocks.reshape(-1, *array.shape)


def whole_of(array, axes, order, dim):
    return in_order(all_blocks(array, axes, order), dim)


def rows_first(arrays, axis, dims):
    turned = [jnp.moveaxis(a, dim, 0) for a, dim in zip(arrays, dims)]
    both = jnp.concatenate([t.reshape(len(t), -1) for t in turned], axis=1)
    result, at, gathered = (lax.all_gather(both, axis, axis=0, tiled=True), 0, [])
    for t, dim in zip(turned, dims):
        piece = result[:, at : at + t[0].size].reshape(-1, *t.shape[1:])
        gathered.append(jnp.moveaxis(piece, 0, dim))
        at += t[0].size
    return tuple(gathered)


def in_blocks(array, dim, count):
    before, after = (array.shape[:dim], array.shape[dim + 1 :])
    return jnp.moveaxis(array.reshape(*before, count, -1, *after), dim, 0)


def summed_on_arrival(array, axis, dim):
    blocks = in_blocks(array, dim, lax.axis_size(axis))
    arrived = lax.all_to_all(blocks, axis, split_axis=0, concat_axis=0, tiled=True)
    return arrived.astype(jnp.float32).sum(axis=0)


def head_group_norm(joined_output, norm_gains):
    center = joined_output - jnp.mean(joined_output, axis=-1, keepdims=True)
    spread = jnp.mean(center * center, axis=-1, keepdims=True)
    normal = (
        center
        * lax.rsqrt(spread + epsilon)
        * norm_gains.reshape(joined_output.shape[1], joined_output.shape[2])
    )
    return normal.reshape(joined_output.shape[0], -1).astype(jnp.bfloat16)


def softmax_update(
    current,
    query_heads,
    query_gates,
    query_pos,
    key_block,
    value_block,
    gate_block,
    key_pos,
    score_scale,
):
    top_now, total_now, weighted = current
    logits = (
        jnp.einsum("qhd,khd->hqk", query_heads, key_block, preferred_element_type=jnp.float32)
        * score_scale
    )
    logits = logits + query_gates[:, :, None] - gate_block[:, None, :]
    logits = jnp.where(key_pos[None, None, :] <= query_pos[None, :, None], logits, -jnp.inf)
    top_new = jnp.maximum(top_now, jnp.max(logits, axis=-1))
    weights_new = jnp.exp(logits - top_new[:, :, None])
    rescale = jnp.exp(top_now - top_new)
    total_new = total_now * rescale + jnp.sum(weights_new, axis=-1)
    weighted_new = weighted * rescale[:, :, None] + jnp.einsum(
        "hqk,khd->hqd",
        weights_new.astype(jnp.bfloat16),
        value_block,
        preferred_element_type=jnp.float32,
    )
    return (top_new, total_new, weighted_new)


def local(
    tokens,
    norm_gain,
    ret_query_weight,
    ret_key_weight,
    ret_value_weight,
    fox_query_weight,
    fox_key_weight,
    fox_value_weight,
    ret_decay,
    ret_state,
    head_norm_gain,
    fox_gates,
    ret_out_weight,
    fox_out_weight,
):
    sequence_length = tokens.shape[0]
    gathered = collect_2(tokens, "tp", 1)
    widened = gathered.astype(jnp.float32)
    normed = (
        widened
        * lax.rsqrt(jnp.mean(widened * widened, axis=-1, keepdims=True) + epsilon)
        * norm_gain
    ).astype(jnp.bfloat16)
    portions = sent_together(
        (
            ret_query_weight,
            ret_key_weight,
            ret_value_weight,
            fox_query_weight,
            fox_key_weight,
            fox_value_weight,
        ),
        SP,
        0,
        1,
    )
    sums = tuple(
        (jnp.dot(normed, portion, preferred_element_type=jnp.float32) for portion in portions)
    )
    ret_query, ret_key, ret_value, fox_query, fox_key, fox_value = [
        result.astype(jnp.bfloat16) for result in sums
    ]
    ret_heads = ret_decay.shape[0]
    key_size = ret_query.shape[1] // ret_heads
    value_size = ret_value.shape[1] // ret_heads
    place = lax.axis_index(SP)
    offset = place * sequence_length
    queries = ret_query.astype(jnp.float32).reshape(sequence_length, ret_heads, key_size)
    keys_local = ret_key.astype(jnp.float32).reshape(
        sequence_length, ret_heads, key_size
    ) * key_size ** (-0.5)
    values_local = ret_value.astype(jnp.float32).reshape(sequence_length, ret_heads, value_size)
    positions = jnp.arange(sequence_length, dtype=jnp.float32)
    spread = positions[:, None] - positions[None, :]
    within = jnp.where(
        spread[None] >= 0, jnp.exp(jnp.maximum(spread, 0.0)[None] * ret_decay[:, None, None]), 0.0
    )
    leading = jnp.exp((positions + 1.0)[:, None] * ret_decay[None, :])
    trailing = jnp.exp((sequence_length - 1.0 - positions)[:, None] * ret_decay[None, :])
    scores = jnp.einsum("ihd,jhd->hij", queries, keys_local) * within
    inner_value = jnp.einsum("hij,jhe->ihe", scores, values_local)
    summary = jnp.einsum("jhd,jhe->hde", keys_local * trailing[:, :, None], values_local)
    portion = whole_of(summary[None], SP, (0, 1), 0)
    shard_ids = jnp.arange(portion.shape[0], dtype=jnp.int32)
    distance = jnp.maximum(place - shard_ids - 1, 0).astype(jnp.float32) * sequence_length
    weight = jnp.where(
        (shard_ids < place)[:, None], jnp.exp(distance[:, None] * ret_decay[None, :]), 0.0
    )
    before = jnp.einsum("sh,shde->hde", weight, portion)
    entering = jnp.exp(offset.astype(jnp.float32) * ret_decay)[:, None, None] * ret_state + before
    carried_state = jnp.einsum("ihd,hde->ihe", queries, entering) * leading[:, :, None]
    retention_mixed = head_group_norm(inner_value + carried_state, head_norm_gain)
    fox_heads = fox_gates.shape[1]
    head_size = fox_query.shape[1] // fox_heads
    score_scale = head_size ** (-0.5)
    starting = (
        jnp.full((fox_heads, sequence_length), -1e30, jnp.float32),
        jnp.zeros((fox_heads, sequence_length), jnp.float32),
        jnp.zeros((fox_heads, sequence_length, head_size), jnp.float32),
    )
    query_heads = fox_query.reshape(sequence_length, fox_heads, head_size)
    own_gates = lax.dynamic_slice_in_dim(fox_gates, offset, sequence_length, 0).T
    query_pos = offset + jnp.arange(sequence_length, dtype=jnp.int32)
    last_query = offset + sequence_length - 1

    def attend(running, portion, first_key):
        key_rows, value_rows = portion
        count = key_rows.shape[0]
        block_rows = next(
            (candidate for candidate in (2048, 1024, 512) if count % candidate == 0), count
        )

        def advance(state_now, number):
            key_start = first_key + number * block_rows

            def compute(current):
                key_block = lax.dynamic_slice_in_dim(
                    key_rows, number * block_rows, block_rows, 0
                ).reshape(block_rows, fox_heads, head_size)
                value_block = lax.dynamic_slice_in_dim(
                    value_rows, number * block_rows, block_rows, 0
                ).reshape(block_rows, fox_heads, head_size)
                gate_block = lax.dynamic_slice_in_dim(fox_gates, key_start, block_rows, 0).T
                key_pos = key_start + jnp.arange(block_rows, dtype=jnp.int32)
                return softmax_update(
                    current,
                    query_heads,
                    own_gates,
                    query_pos,
                    key_block,
                    value_block,
                    gate_block,
                    key_pos,
                    score_scale,
                )

            def unchanged(current):
                return current

            return (lax.cond(key_start <= last_query, compute, unchanged, state_now), None)

        finished, _ = lax.scan(advance, running, jnp.arange(count // block_rows, dtype=jnp.int32))
        return finished

    top_final, total_final, weighted_final = attend(
        starting, sent_together((fox_key, fox_value), SP, 0, 1), jnp.int32(0)
    )
    fox_mix = (
        jnp.transpose(weighted_final / total_final[:, :, None], (1, 0, 2))
        .reshape(sequence_length, fox_heads * head_size)
        .astype(jnp.bfloat16)
    )
    ret_full, fox_full = rows_first((ret_out_weight, fox_out_weight), SP, (1, 1))
    mixed = summed_on_arrival(
        (
            jnp.dot(retention_mixed, ret_full, preferred_element_type=jnp.float32)
            + jnp.dot(fox_mix, fox_full, preferred_element_type=jnp.float32)
        ).astype(jnp.bfloat16),
        "tp",
        0,
    )
    return mixed.astype(jnp.bfloat16)


def solution(mesh):
    torus = Mesh(
        mesh.devices.reshape(mesh.shape["grp"], 32, 2, mesh.shape["tp"]),
        ("grp", "sp_0", "sp_1", "tp"),
    )
    return jax.shard_map(
        local,
        mesh=torus,
        in_specs=(
            P(GRP_SP, "tp"),
            P(),
            P(SP, "tp"),
            P(SP, "tp"),
            P(SP, "tp"),
            P(SP, "tp"),
            P(SP, "tp"),
            P(SP, "tp"),
            P("tp"),
            P(("grp", "tp"), None, None),
            P("tp"),
            P("grp", "tp"),
            P("tp", SP),
            P("tp", SP),
        ),
        out_specs=P(GRP_SP_TP, None),
        check_vma=False,
    )
```

profile of v0, /device:TPU:1824, one launch (start us, length us, event | category | flops | bytes accessed | tf_op | source)
XLA Modules:
  0.0 499.1 jit_solution(9401134259431210037)
XLA Ops:
  6.6 1.5 concatenate.9
  10.3 4.6 all-to-all-start
  15.7 14.3 %all-to-all-done = bf16[4,256,512]{1,2,0:T(8,128)(2,1)S(1)} async-done(((bf16[4,256,512]{1,2,0:T(8,128)(2,1)}), bf16[4,256,512]{1,2,0:T(8,128)(2,1)S(1)}, u32[]{:S(2)}, u32[]{:S(2)}) %all-to-all-start) | async-done | bytes 1048608 | tf_op jit(solution)/shard_map/all_to_all | solution.py:21
  30.7 99.2 %all-gather.6.cloned.1.call-done = bf16[2048,640]{1,0:T(8,128)(2,1)} async-done(((bf16[32,640]{1,0:T(8,128)(2,1)}), bf16[2048,640]{1,0:T(8,128)(2,1)}) %all-gather.6.cloned.1.call-update) | async-done | bytes 2621456 | tf_op jit(solution)/shard_map/all_gather | solution.py:33
  134.7 1.6 convolution_convert_fusion.4
  137.9 56.2 %all-gather = bf16[64,32,64]{2,1,0:T(8,128)(2,1)S(1)} all-gather(bf16[2,32,64]{2,1,0:T(8,128)(2,1)S(1)} %fusion.37), channel_id=2, replica_groups=mesh['grp'=2,'sp_0'=32,'sp_1'=2,'tp'=4] {'sp_0'}, dimensions={0}, use_global_device_ids=true | all-gather | bytes 270336 | tf_op jit(solution)/shard_map/all_gather | solution.py:40
  194.0 2.6 all-gather.1
  199.6 1.4 convolution_convert_fusion
  201.0 56.6 %all-gather.8.cloned.1.call-done = bf16[2048,256]{1,0:T(8,128)(2,1)} async-done(((bf16[32,256]{1,0:T(8,128)(2,1)}), bf16[2048,256]{1,0:T(8,128)(2,1)}) %all-gather.8.cloned.1.call-update) | async-done | bytes 1048592 | tf_op jit(solution)/shard_map/all_gather | solution.py:54
  257.7 1.5 fusion.23
  259.2 148.0 %all-gather.10.cloned.1.call-done = bf16[16384,256]{0,1:T(8,128)(2,1)} async-done(((bf16[256,256]{0,1:T(8,128)(2,1)}), bf16[16384,256]{0,1:T(8,128)(2,1)}) %all-gather.10.cloned.1.call-update) | async-done | bytes 8388624 | tf_op jit(solution)/shard_map/all_gather | solution.py:33
  407.2 5.8 %fusion.48 = (bf16[16384,128]{0,1:T(8,128)(2,1)}, bf16[16384,128]{0,1:T(8,128)(2,1)}) fusion(bf16[16384,256]{0,1:T(8,128)(2,1)} %all-gather.10.cloned.1.call-done), kind=kLoop, calls=%fused_computation.83 | loop fusion | bytes 16777216 | tf_op jit(solution)/shard_map/split | solution.py:34
  413.0 58.6 %while.15 = (s32[]{:T(128)}, f32[2,256]{1,0:T(2,128)S(1)}, f32[2,256]{1,0:T(2,128)S(1)}, f32[2,256,64]{1,2,0:T(8,128)S(1)}, s32[8]{0:T(128)S(1)}, /*index=5*/s32...) while((s32[]{:T(128)}, f32[2,256]{1,0:T(2,128)S(1)}, ...), condition=%wide.region_8.9_spmd.clone, body=%wide.region_3.8_spmd.clone.sunk | while | flops 278465792 | bytes 17209772 | solution.py:237
  414.3 6.0 %conditional.3 = ((f32[2,256]{1,0:T(2,128)S(1)}, f32[2,256]{1,0:T(2,128)S(1)}, f32[2,256,64]{1,2,0:T(8,128)S(1)})) conditional(s32[]{:T(128)} %convert_element_type.113, (f32[2,256]{1,0:T(2,128)S(1)}, f32[2,256]{1,0:T(2,128)S(1)}, f32[2,256,64]{1,2,0:T(8,128)S(1)}) %tuple.39, (s32[]{:T(128)}, s32[]{:T(128)}, s32[]{:T(128)}, ...), branch_computations={%region_4.4_spmd, %region_5.7_spmd} | conditional | flops 278465792 | bytes 17208448 | solution.py:235
  421.6 6.1 %conditional.3 = ((f32[2,256]{1,0:T(2,128)S(1)}, f32[2,256]{1,0:T(2,128)S(1)}, f32[2,256,64]{1,2,0:T(8,128)S(1)})) conditional(s32[]{:T(128)} %convert_element_type.113, (f32[2,256]{1,0:T(2,128)S(1)}, f32[2,256]{1,0:T(2,128)S(1)}, f32[2,256,64]{1,2,0:T(8,128)S(1)}) %tuple.39, (s32[]{:T(128)}, s32[]{:T(128)}, s32[]{:T(128)}, ...), branch_computations={%region_4.4_spmd, %region_5.7_spmd} | conditional | flops 278465792 | bytes 17208448 | solution.py:235
  424.9 1.4 fusion.47
  429.0 6.0 %conditional.3 = ((f32[2,256]{1,0:T(2,128)S(1)}, f32[2,256]{1,0:T(2,128)S(1)}, f32[2,256,64]{1,2,0:T(8,128)S(1)})) conditional(s32[]{:T(128)} %convert_element_type.113, (f32[2,256]{1,0:T(2,128)S(1)}, f32[2,256]{1,0:T(2,128)S(1)}, f32[2,256,64]{1,2,0:T(8,128)S(1)}) %tuple.39, (s32[]{:T(128)}, s32[]{:T(128)}, s32[]{:T(128)}, ...), branch_computations={%region_4.4_spmd, %region_5.7_spmd} | conditional | flops 278465792 | bytes 17208448 | solution.py:235
  436.3 6.1 %conditional.3 = ((f32[2,256]{1,0:T(2,128)S(1)}, f32[2,256]{1,0:T(2,128)S(1)}, f32[2,256,64]{1,2,0:T(8,128)S(1)})) conditional(s32[]{:T(128)} %convert_element_type.113, (f32[2,256]{1,0:T(2,128)S(1)}, f32[2,256]{1,0:T(2,128)S(1)}, f32[2,256,64]{1,2,0:T(8,128)S(1)}) %tuple.39, (s32[]{:T(128)}, s32[]{:T(128)}, s32[]{:T(128)}, ...), branch_computations={%region_4.4_spmd, %region_5.7_spmd} | conditional | flops 278465792 | bytes 17208448 | solution.py:235
  439.6 1.4 fusion.47
  443.6 6.0 %conditional.3 = ((f32[2,256]{1,0:T(2,128)S(1)}, f32[2,256]{1,0:T(2,128)S(1)}, f32[2,256,64]{1,2,0:T(8,128)S(1)})) conditional(s32[]{:T(128)} %convert_element_type.113, (f32[2,256]{1,0:T(2,128)S(1)}, f32[2,256]{1,0:T(2,128)S(1)}, f32[2,256,64]{1,2,0:T(8,128)S(1)}) %tuple.39, (s32[]{:T(128)}, s32[]{:T(128)}, s32[]{:T(128)}, ...), branch_computations={%region_4.4_spmd, %region_5.7_spmd} | conditional | flops 278465792 | bytes 17208448 | solution.py:235
  451.0 6.1 %conditional.3 = ((f32[2,256]{1,0:T(2,128)S(1)}, f32[2,256]{1,0:T(2,128)S(1)}, f32[2,256,64]{1,2,0:T(8,128)S(1)})) conditional(s32[]{:T(128)} %convert_element_type.113, (f32[2,256]{1,0:T(2,128)S(1)}, f32[2,256]{1,0:T(2,128)S(1)}, f32[2,256,64]{1,2,0:T(8,128)S(1)}) %tuple.39, (s32[]{:T(128)}, s32[]{:T(128)}, s32[]{:T(128)}, ...), branch_computations={%region_4.4_spmd, %region_5.7_spmd} | conditional | flops 278465792 | bytes 17208448 | solution.py:235
  458.3 6.0 %conditional.3 = ((f32[2,256]{1,0:T(2,128)S(1)}, f32[2,256]{1,0:T(2,128)S(1)}, f32[2,256,64]{1,2,0:T(8,128)S(1)})) conditional(s32[]{:T(128)} %convert_element_type.113, (f32[2,256]{1,0:T(2,128)S(1)}, f32[2,256]{1,0:T(2,128)S(1)}, f32[2,256,64]{1,2,0:T(8,128)S(1)}) %tuple.39, (s32[]{:T(128)}, s32[]{:T(128)}, s32[]{:T(128)}, ...), branch_computations={%region_4.4_spmd, %region_5.7_spmd} | conditional | flops 278465792 | bytes 17208448 | solution.py:235
  465.6 6.0 %conditional.3 = ((f32[2,256]{1,0:T(2,128)S(1)}, f32[2,256]{1,0:T(2,128)S(1)}, f32[2,256,64]{1,2,0:T(8,128)S(1)})) conditional(s32[]{:T(128)} %convert_element_type.113, (f32[2,256]{1,0:T(2,128)S(1)}, f32[2,256]{1,0:T(2,128)S(1)}, f32[2,256,64]{1,2,0:T(8,128)S(1)}) %tuple.39, (s32[]{:T(128)}, s32[]{:T(128)}, s32[]{:T(128)}, ...), branch_computations={%region_4.4_spmd, %region_5.7_spmd} | conditional | flops 278465792 | bytes 17208448 | solution.py:235
  472.2 19.4 %all_to_all.10 = bf16[4,64,2048]{2,1,0:T(8,128)(2,1)S(1)} all-to-all(bf16[4,64,2048]{2,1,0:T(8,128)(2,1)S(1)} %bitcast.68), channel_id=1, replica_groups=mesh['grp'=2,'sp_0'=32,'sp_1'=2,'tp'=4] {'tp'}, dimensions={0} | all-to-all | bytes 2097152 | tf_op jit(solution)/shard_map/all_to_all | solution.py:69
  (160 shorter events, 58.8 us)
Async XLA Ops:
  6.5 8.3 %copy-start.3 = (bf16[128,32]{0,1:T(8,128)(2,1)S(1)}, bf16[128,32]{0,1:T(8,128)(2,1)}, u32[]{:S(2)}) copy-start(bf16[128,32]{0,1:T(8,128)(2,1)} %param.31) | copy-start | bytes 24580
  6.5 8.3 %copy-start.4 = (bf16[128,32]{0,1:T(8,128)(2,1)S(1)}, bf16[128,32]{0,1:T(8,128)(2,1)}, u32[]{:S(2)}) copy-start(bf16[128,32]{0,1:T(8,128)(2,1)} %param.30) | copy-start | bytes 24580
  6.6 23.8 %copy-start.2 = (f32[2048]{0:T(1024)S(1)}, f32[2048]{0:T(1024)}, u32[]{:S(2)}) copy-start(f32[2048]{0:T(1024)} %param.19) | copy-start | bytes 24580
  6.6 123.3 %all-gather.6.cloned.1.call-start = ((), (), s32[]{:S(2)}) async-start(), calls=%async_computation.2 | async-start | bytes 2662400 | tf_op jit(solution)/shard_map/all_gather | solution.py:33
  10.3 19.7 %all-to-all-start = ((bf16[4,256,512]{1,2,0:T(8,128)(2,1)}), bf16[4,256,512]{1,2,0:T(8,128)(2,1)S(1)}, u32[]{:S(2)}, u32[]{:S(2)}) async-start(bf16[4,256,512]{1,2,0:T(8,128)(2,1)} %broadcast_in_dim.40), calls=%async_computation | async-start | bytes 2097152 | tf_op jit(solution)/shard_map/all_to_all | solution.py:21
  14.8 242.8 %all-gather.8.cloned.1.call-start = ((), (), s32[]{:S(2)}) async-start(), calls=%async_computation.3 | async-start | bytes 1064960 | tf_op jit(solution)/shard_map/all_gather | solution.py:54
  15.6 391.6 %all-gather.10.cloned.1.call-start = ((), (), s32[]{:S(2)}) async-start(), calls=%async_computation.4 | async-start | bytes 8519680 | tf_op jit(solution)/shard_map/all_gather | solution.py:33
  30.3 103.1 %copy-start.6 = (f32[128]{0:T(128)S(1)}, f32[128]{0:T(128)}, u32[]{:S(2)}) copy-start(f32[128]{0:T(128)} %param.28) | copy-start | bytes 1540
  30.3 103.2 %copy-start.5 = (f32[2]{0:T(128)S(1)}, f32[2]{0:T(128)}, u32[]{:S(2)}) copy-start(f32[2]{0:T(128)} %param.26) | copy-start | bytes 28
  196.6 2.1 copy-start.1
  413.0 58.7 %copy-start = (bf16[2048,256]{1,0:T(8,128)(2,1)S(1)}, bf16[2048,256]{1,0:T(8,128)(2,1)}, u32[]{:S(2)}) copy-start(bf16[2048,256]{1,0:T(8,128)(2,1)} %all-gather.8.cloned.1.call-done) | copy-start | bytes 3145732
Sparse Core Ops, SparseCore 0:
  9.5 120.3 all-gather.5
  132.0 125.5 all-gather.7
  259.7 147.4 all-gather.9
where the time goes:
time: 501 us; the launch traced here: 499 us
  waiting for transfers between devices  318 us (63%)
  blocking collectives  78.2 us (16%)
  local copies, waits for them, and re-layouts  31.8 us (6%)
  matrix products  29.6 us (6%)
  between operations  13.3 us (3%)
  other arithmetic  11.7 us (2%)
  loops' own time  11.4 us (2%)
    all_gather x2, waiting for transfers between devices, sent_together(): result = lax.all_gather(both, axis, axis=dim, tiled=True)  247 us
    all_gather x2, blocking collectives, all_blocks(): blocks = lax.all_gather(blocks, axes[k])  58.8 us
    all_gather x1, waiting for transfers between devices, rows_first(): lax.all_gather(both, axis, axis=0, tiled=True)  56.6 us
    all_to_all x1, blocking collectives, summed_on_arrival(): lax.all_to_all(blocks, axis, split_axis=0, concat_axis=0, tiled=True)  19.4 us
    all_to_all x1, waiting for transfers between devices, from_everyone(): lax.all_to_all(jnp.broadcast_to(array[None], (count, *array.shape)), axis...  14.3 us
    dot_general x8, matrix products, softmax_update(): jnp.einsum('qhd,khd->hqk', query_heads, key_block, preferred_element_type...  11.2 us
    dynamic_slice x8, local copies, waits for them, and re-layouts, compute(): lax.dynamic_slice_in_dim(value_rows, number * block_rows, block_rows, 0)  10.2 us
  transfers between devices with their start and end apart: 4, of which 4 were waited for; matrix products, arithmetic and copies ran while one was open for 3% of the time, Pallas kernels for 0%

commit v1 on v0

--- a/solution.py
+++ b/solution.py
@@ -51,7 +51,13 @@
 def rows_first(arrays, axis, dims):
     turned = [jnp.moveaxis(a, dim, 0) for a, dim in zip(arrays, dims)]
     both = jnp.concatenate([t.reshape(len(t), -1) for t in turned], axis=1)
-    result, at, gathered = (lax.all_gather(both, axis, axis=0, tiled=True), 0, [])
+    result, at, gathered = (
+        jnp.concatenate(
+            lax.all_to_all(jnp.stack([both] * lax.axis_size(axis)), axis, 0, 0), axis=0
+        ),
+        0,
+        [],
+    )
     for t, dim in zip(turned, dims):
         piece = result[:, at : at + t[0].size].reshape(-1, *t.shape[1:])
         gathered.append(jnp.moveaxis(piece, 0, dim))

time: 501 us -> 453 us (0.904)
  the two profiles are of different devices: /device:TPU:1824 before, /device:TPU:1888 now
where the time goes in v1:
time: 453 us; the launch traced here: 452 us
  blocking collectives  192 us (42%)
  waiting for transfers between devices  146 us (32%)
  local copies, waits for them, and re-layouts  31.9 us (7%)
  matrix products  28.5 us (6%)
  starting transfers between devices  17.4 us (4%)
  between operations  13.7 us (3%)
  loops' own time  11.4 us (3%)
  other arithmetic  11.1 us (2%)
    all_gather x2, blocking collectives, all_blocks(): blocks = lax.all_gather(blocks, axes[k])  150 us
    all_gather x2, waiting for transfers between devices, sent_together(): result = lax.all_gather(both, axis, axis=dim, tiled=True)  146 us
    all_to_all x1, blocking collectives, summed_on_arrival(): lax.all_to_all(blocks, axis, split_axis=0, concat_axis=0, tiled=True)  22 us
    all_to_all x1, blocking collectives, from_everyone(): lax.all_to_all(jnp.broadcast_to(array[None], (count, *array.shape)), axis...  19.5 us
    all_to_all x1, starting transfers between devices, rows_first(): lax.all_to_all(jnp.stack([both] * lax.axis_size(axis)), axis, 0, 0)  17.4 us
    dot_general x8, matrix products, softmax_update(): jnp.einsum('qhd,khd->hqk', query_heads, key_block, preferred_element_type...  11.2 us
    dynamic_slice x8, local copies, waits for them, and re-layouts, compute(): lax.dynamic_slice_in_dim(value_rows, number * block_rows, block_rows, 0)  10.2 us
  transfers between devices with their start and end apart: 3, of which 2 were waited for; matrix products, arithmetic and copies ran while one was open for 3% of the time, Pallas kernels for 0%

profile of v1, /device:TPU:1888, one launch (start us, length us, event | category | flops | bytes accessed | tf_op | source)
XLA Modules:
  0.0 451.7 jit_solution(16841999052273598982)
XLA Ops:
  6.6 1.5 concatenate.9
  9.3 19.5 %all_to_all.15 = bf16[4,256,512]{1,2,0:T(8,128)(2,1)S(1)} all-to-all(bf16[4,256,512]{1,2,0:T(8,128)(2,1)S(1)} %broadcast_in_dim.40), channel_id=1, replica_groups=mesh['grp'=2,'sp_0'=32,'sp_1'=2,'tp'=4] {'tp'}, dimensions={0} | all-to-all | bytes 2097152 | tf_op jit(solution)/shard_map/all_to_all | solution.py:21
  29.6 99.5 %all-gather.5.cloned.1.call-done = bf16[2048,640]{1,0:T(8,128)(2,1)} async-done(((bf16[32,640]{1,0:T(8,128)(2,1)}), bf16[2048,640]{1,0:T(8,128)(2,1)}) %all-gather.5.cloned.1.call-update) | async-done | bytes 2621456 | tf_op jit(solution)/shard_map/all_gather | solution.py:33
  130.5 1.4 convolution_convert_fusion.2
  133.8 17.4 %all-to-all-start.1 = ((bf16[64,32,256]{2,1,0:T(8,128)(2,1)}), bf16[64,32,256]{2,1,0:T(8,128)(2,1)S(1)}, u32[]{:S(2)}, u32[]{:S(2)}) async-start(bf16[64,32,256]{2,1,0:T(8,128)(2,1)} %stack.2), calls=%async_computation.1 | async-start | bytes 2097152 | tf_op jit(solution)/shard_map/all_to_all | solution.py:56
  152.4 1.6 convolution_convert_fusion.4
  155.6 147.4 %all-gather = bf16[64,32,64]{2,1,0:T(8,128)(2,1)S(1)} all-gather(bf16[2,32,64]{2,1,0:T(8,128)(2,1)S(1)} %fusion.37), channel_id=2, replica_groups=mesh['grp'=2,'sp_0'=32,'sp_1'=2,'tp'=4] {'sp_0'}, dimensions={0}, use_global_device_ids=true | all-gather | bytes 270336 | tf_op jit(solution)/shard_map/all_gather | solution.py:40
  303.0 2.7 all-gather.1
  310.5 46.4 %all-gather.7.cloned.1.call-done = bf16[16384,256]{0,1:T(8,128)(2,1)} async-done(((bf16[256,256]{0,1:T(8,128)(2,1)}), bf16[16384,256]{0,1:T(8,128)(2,1)}) %all-gather.7.cloned.1.call-update) | async-done | bytes 8388624 | tf_op jit(solution)/shard_map/all_gather | solution.py:33
  356.9 5.8 %fusion.48 = (bf16[16384,128]{0,1:T(8,128)(2,1)}, bf16[16384,128]{0,1:T(8,128)(2,1)}) fusion(bf16[16384,256]{0,1:T(8,128)(2,1)} %all-gather.7.cloned.1.call-done), kind=kLoop, calls=%fused_computation.83 | loop fusion | bytes 16777216 | tf_op jit(solution)/shard_map/split | solution.py:34
  362.8 58.6 %while.15 = (s32[]{:T(128)}, f32[2,256]{1,0:T(2,128)S(1)}, f32[2,256]{1,0:T(2,128)S(1)}, f32[2,256,64]{1,2,0:T(8,128)S(1)}, s32[8]{0:T(128)S(1)}, /*index=5*/s32...) while((s32[]{:T(128)}, f32[2,256]{1,0:T(2,128)S(1)}, ...), condition=%wide.region_8.9_spmd.clone, body=%wide.region_3.8_spmd.clone.sunk | while | flops 278465792 | bytes 17209772 | solution.py:243
  364.0 6.1 %conditional.3 = ((f32[2,256]{1,0:T(2,128)S(1)}, f32[2,256]{1,0:T(2,128)S(1)}, f32[2,256,64]{1,2,0:T(8,128)S(1)})) conditional(s32[]{:T(128)} %convert_element_type.113, (f32[2,256]{1,0:T(2,128)S(1)}, f32[2,256]{1,0:T(2,128)S(1)}, f32[2,256,64]{1,2,0:T(8,128)S(1)}) %tuple.39, (s32[]{:T(128)}, s32[]{:T(128)}, s32[]{:T(128)}, ...), branch_computations={%region_4.4_spmd, %region_5.7_spmd} | conditional | flops 278465792 | bytes 17208448 | solution.py:241
  367.3 1.4 fusion.47
  371.4 6.1 %conditional.3 = ((f32[2,256]{1,0:T(2,128)S(1)}, f32[2,256]{1,0:T(2,128)S(1)}, f32[2,256,64]{1,2,0:T(8,128)S(1)})) conditional(s32[]{:T(128)} %convert_element_type.113, (f32[2,256]{1,0:T(2,128)S(1)}, f32[2,256]{1,0:T(2,128)S(1)}, f32[2,256,64]{1,2,0:T(8,128)S(1)}) %tuple.39, (s32[]{:T(128)}, s32[]{:T(128)}, s32[]{:T(128)}, ...), branch_computations={%region_4.4_spmd, %region_5.7_spmd} | conditional | flops 278465792 | bytes 17208448 | solution.py:241
  374.6 1.4 fusion.47
  378.7 6.0 %conditional.3 = ((f32[2,256]{1,0:T(2,128)S(1)}, f32[2,256]{1,0:T(2,128)S(1)}, f32[2,256,64]{1,2,0:T(8,128)S(1)})) conditional(s32[]{:T(128)} %convert_element_type.113, (f32[2,256]{1,0:T(2,128)S(1)}, f32[2,256]{1,0:T(2,128)S(1)}, f32[2,256,64]{1,2,0:T(8,128)S(1)}) %tuple.39, (s32[]{:T(128)}, s32[]{:T(128)}, s32[]{:T(128)}, ...), branch_computations={%region_4.4_spmd, %region_5.7_spmd} | conditional | flops 278465792 | bytes 17208448 | solution.py:241
  386.0 6.1 %conditional.3 = ((f32[2,256]{1,0:T(2,128)S(1)}, f32[2,256]{1,0:T(2,128)S(1)}, f32[2,256,64]{1,2,0:T(8,128)S(1)})) conditional(s32[]{:T(128)} %convert_element_type.113, (f32[2,256]{1,0:T(2,128)S(1)}, f32[2,256]{1,0:T(2,128)S(1)}, f32[2,256,64]{1,2,0:T(8,128)S(1)}) %tuple.39, (s32[]{:T(128)}, s32[]{:T(128)}, s32[]{:T(128)}, ...), branch_computations={%region_4.4_spmd, %region_5.7_spmd} | conditional | flops 278465792 | bytes 17208448 | solution.py:241
  389.3 1.4 fusion.47
  393.4 6.0 %conditional.3 = ((f32[2,256]{1,0:T(2,128)S(1)}, f32[2,256]{1,0:T(2,128)S(1)}, f32[2,256,64]{1,2,0:T(8,128)S(1)})) conditional(s32[]{:T(128)} %convert_element_type.113, (f32[2,256]{1,0:T(2,128)S(1)}, f32[2,256]{1,0:T(2,128)S(1)}, f32[2,256,64]{1,2,0:T(8,128)S(1)}) %tuple.39, (s32[]{:T(128)}, s32[]{:T(128)}, s32[]{:T(128)}, ...), branch_computations={%region_4.4_spmd, %region_5.7_spmd} | conditional | flops 278465792 | bytes 17208448 | solution.py:241
  400.7 6.1 %conditional.3 = ((f32[2,256]{1,0:T(2,128)S(1)}, f32[2,256]{1,0:T(2,128)S(1)}, f32[2,256,64]{1,2,0:T(8,128)S(1)})) conditional(s32[]{:T(128)} %convert_element_type.113, (f32[2,256]{1,0:T(2,128)S(1)}, f32[2,256]{1,0:T(2,128)S(1)}, f32[2,256,64]{1,2,0:T(8,128)S(1)}) %tuple.39, (s32[]{:T(128)}, s32[]{:T(128)}, s32[]{:T(128)}, ...), branch_computations={%region_4.4_spmd, %region_5.7_spmd} | conditional | flops 278465792 | bytes 17208448 | solution.py:241
  403.9 1.4 fusion.47
  408.0 6.0 %conditional.3 = ((f32[2,256]{1,0:T(2,128)S(1)}, f32[2,256]{1,0:T(2,128)S(1)}, f32[2,256,64]{1,2,0:T(8,128)S(1)})) conditional(s32[]{:T(128)} %convert_element_type.113, (f32[2,256]{1,0:T(2,128)S(1)}, f32[2,256]{1,0:T(2,128)S(1)}, f32[2,256,64]{1,2,0:T(8,128)S(1)}) %tuple.39, (s32[]{:T(128)}, s32[]{:T(128)}, s32[]{:T(128)}, ...), branch_computations={%region_4.4_spmd, %region_5.7_spmd} | conditional | flops 278465792 | bytes 17208448 | solution.py:241
  415.3 6.0 %conditional.3 = ((f32[2,256]{1,0:T(2,128)S(1)}, f32[2,256]{1,0:T(2,128)S(1)}, f32[2,256,64]{1,2,0:T(8,128)S(1)})) conditional(s32[]{:T(128)} %convert_element_type.113, (f32[2,256]{1,0:T(2,128)S(1)}, f32[2,256]{1,0:T(2,128)S(1)}, f32[2,256,64]{1,2,0:T(8,128)S(1)}) %tuple.39, (s32[]{:T(128)}, s32[]{:T(128)}, s32[]{:T(128)}, ...), branch_computations={%region_4.4_spmd, %region_5.7_spmd} | conditional | flops 278465792 | bytes 17208448 | solution.py:241
  421.9 22.0 %all_to_all.16 = bf16[4,64,2048]{2,1,0:T(8,128)(2,1)S(1)} all-to-all(bf16[4,64,2048]{2,1,0:T(8,128)(2,1)S(1)} %bitcast.69), channel_id=1, replica_groups=mesh['grp'=2,'sp_0'=32,'sp_1'=2,'tp'=4] {'tp'}, dimensions={0} | all-to-all | bytes 2097152 | tf_op jit(solution)/shard_map/all_to_all | solution.py:75
  (157 shorter events, 55.8 us)
Async XLA Ops:
  6.5 22.7 %copy-start.1 = (f32[2048]{0:T(1024)S(1)}, f32[2048]{0:T(1024)}, u32[]{:S(2)}) copy-start(f32[2048]{0:T(1024)} %param.19) | copy-start | bytes 24580
  6.5 122.5 %all-gather.5.cloned.1.call-start = ((), (), s32[]{:S(2)}) async-start(), calls=%async_computation.3 | async-start | bytes 2662400 | tf_op jit(solution)/shard_map/all_gather | solution.py:33
  8.1 348.8 %all-gather.7.cloned.1.call-start = ((), (), s32[]{:S(2)}) async-start(), calls=%async_computation.4 | async-start | bytes 8519680 | tf_op jit(solution)/shard_map/all_gather | solution.py:33
  29.2 103.4 %copy-start.2 = (bf16[128,32]{0,1:T(8,128)(2,1)S(1)}, bf16[128,32]{0,1:T(8,128)(2,1)}, u32[]{:S(2)}) copy-start(bf16[128,32]{0,1:T(8,128)(2,1)} %param.31) | copy-start | bytes 24580
  29.2 103.4 %copy-start.3 = (bf16[128,32]{0,1:T(8,128)(2,1)S(1)}, bf16[128,32]{0,1:T(8,128)(2,1)}, u32[]{:S(2)}) copy-start(bf16[128,32]{0,1:T(8,128)(2,1)} %param.30) | copy-start | bytes 24580
  130.5 20.7 %copy-start.5 = (f32[128]{0:T(128)S(1)}, f32[128]{0:T(128)}, u32[]{:S(2)}) copy-start(f32[128]{0:T(128)} %param.28) | copy-start | bytes 1540
  130.5 20.8 %copy-start.4 = (f32[2]{0:T(128)S(1)}, f32[2]{0:T(128)}, u32[]{:S(2)}) copy-start(f32[2]{0:T(128)} %param.26) | copy-start | bytes 28
  133.8 176.3 %all-to-all-start.1 = ((bf16[64,32,256]{2,1,0:T(8,128)(2,1)}), bf16[64,32,256]{2,1,0:T(8,128)(2,1)S(1)}, u32[]{:S(2)}, u32[]{:S(2)}) async-start(bf16[64,32,256]{2,1,0:T(8,128)(2,1)} %stack.2), calls=%async_computation.1 | async-start | bytes 2097152 | tf_op jit(solution)/shard_map/all_to_all | solution.py:56
  305.7 2.1 copy-start
Sparse Core Ops, SparseCore 0:
  9.5 119.5 all-gather.4
  132.7 224.1 all-gather.6
